TPU v7x, 512 devices: a whole 4x4x16 slice. The times are simulated.
512 devices in a mesh: fs: 16 (over y, x), tp: 32 (over z, core).
Axes of the slice: x: 4, y: 4, z: 16, core: 2. Of those that a mesh axis runs over, the one named last changes fastest.
Arguments:
- prompt: bfloat16 [65536, 2048], P(('fs', 'tp')), may hold values from -6 to 6
- norm_gain: float32 [2048], P('tp'), may hold values from 0.1 to 1.9
- gate_master: float32 [32, 2, 512, 2048], P(None, None, 'fs', 'tp'), may hold values from -0.125 to 0.125
- up_master: float32 [32, 2, 512, 2048], P(None, None, 'fs', 'tp'), may hold values from -0.125 to 0.125
- down_master: float32 [32, 2, 512, 2048], P(None, None, 'fs', 'tp'), may hold values from -0.25 to 0.25
- group_pick: int32 [65536, 1], P(('fs', 'tp')), may hold values from 0 to 31; in each aligned block of 128 rows (0 to 127, 128 to 255, ...) at most 8 rows name the same one
- route_weight: bfloat16 [65536, 2], P(('fs', 'tp')), may hold values from 0.099609375 to 1
Outputs:
- gate_serve: bfloat16 [32, 2, 512, 2048], P('tp', None, 'fs')
- up_serve: bfloat16 [32, 2, 512, 2048], P('tp', None, 'fs')
- down_serve: bfloat16 [32, 2, 512, 2048], P('tp', None, 'fs')
- mixed: bfloat16 [65536, 2048], P(('fs', 'tp'))
Inputs may be any that keep to these rules, and one draw needn't show every extreme that they name: `group_pick`: in the rows of one device no group is named by more than 8 rows, and in every draw some device's rows name one group exactly 8 times.
All inputs are finite; a program needn't handle non-finite values.
Results may differ from a plain program's by a relative error of at most 0.0081.
Values may be sent and summed in bfloat16 or wider, within the bound.
A program may use at most 64 MiB of HBM per device.

v0:
```python
import jax
import jax.numpy as jnp
from jax import lax
from jax.sharding import Mesh
from jax.sharding import PartitionSpec as P

TP = ("tp_0", "tp_1")
FS_TP = ("fs", "tp_0", "tp_1")


EPS = 1e-06


def sent_together(arrays, axis, split_dim, concat_dim, along):
    widths = [a.shape[along] for a in arrays]
    both = jnp.concatenate(arrays, axis=along)
    out = lax.all_to_all(both, axis, split_axis=split_dim, concat_axis=concat_dim, tiled=True)
    return tuple(jnp.split(out, [sum(widths[:k]) for k in range(1, len(widths))], axis=along))


def sent_together_2(arrays, axis, dim, along):
    widths = [a.shape[along] for a in arrays]
    both = jnp.concatenate(arrays, axis=along)
    out = lax.all_gather(both, axis, axis=dim, tiled=True)
    return tuple(jnp.split(out, [sum(widths[:k]) for k in range(1, len(widths))], axis=along))


def split_up(shard, dim, length):
    before, after = (shard.shape[:dim], shard.shape[dim + 1 :])
    return jnp.moveaxis(shard.reshape(*before, length, -1, *after), dim, 0)


def laid_out(tiles, dim):
    lengths = list(tiles.shape[1:])
    lengths[dim] *= tiles.shape[0]
    return jnp.moveaxis(tiles, 0, dim).reshape(lengths)


def moved_by_axis(tiles, axes, turns):
    inside = tiles.shape[1:]
    out = tiles.reshape(*(lax.axis_size(a) for a in axes), *inside)
    for k in turns:
        out = lax.all_to_all(out, axes[k], k, k, tiled=True)
    return out.reshape(-1, *inside)


def exchange_by_chip(shard, groups, turns, split_dim, concat_dim):
    length = lax.axis_size(groups[0]) * lax.axis_size(groups[1])
    tiles = split_up(shard, split_dim, length)
    return laid_out(moved_by_axis(tiles, groups, turns), concat_dim)


def expert_rows(group_rows, weights, pieces):
    gate_piece, up_piece, down_piece = pieces
    expert_count = gate_piece.shape[1]
    unit_count = gate_piece.shape[2]
    model_width = gate_piece.shape[3]
    row_count = group_rows.shape[0]
    gate_matrix = gate_piece.reshape(expert_count * unit_count, model_width)
    up_matrix = up_piece.reshape(expert_count * unit_count, model_width)
    down_matrix = down_piece.reshape(expert_count * unit_count, model_width)
    gate_pre = jnp.einsum("sd,hd->sh", group_rows, gate_matrix, preferred_element_type=jnp.float32)
    up_pre = jnp.einsum("sd,hd->sh", group_rows, up_matrix, preferred_element_type=jnp.float32)
    active = (jax.nn.silu(gate_pre) * up_pre).reshape(row_count, expert_count, unit_count)
    hidden = (weights.astype(jnp.float32)[:, :, None] * active).reshape(
        row_count, expert_count * unit_count
    )
    hidden = hidden.astype(jnp.bfloat16)
    return jnp.dot(hidden, down_matrix, preferred_element_type=jnp.float32)


def per_device(prompt, norm_gain, gate_master, up_master, down_master, group_pick, route_weight):
    group_total = lax.axis_size(TP)
    gate_local = (gate_master * norm_gain).astype(jnp.bfloat16)
    up_local = (up_master * norm_gain).astype(jnp.bfloat16)
    down_local = down_master.astype(jnp.bfloat16)
    gate_serve, up_serve, down_serve = sent_together(
        (gate_local, up_local, down_local), TP, 0, 3, 1
    )
    values = prompt.astype(jnp.float32)
    normed = (values * lax.rsqrt(jnp.mean(values * values, axis=1, keepdims=True) + EPS)).astype(
        jnp.bfloat16
    )
    tok_count = prompt.shape[0]
    capacity = 2 * tok_count // group_total
    slot_total = group_total * capacity
    chosen = group_pick[:, 0]
    member = (chosen[:, None] == jnp.arange(group_total, dtype=jnp.int32)[None, :]).astype(
        jnp.int32
    )
    slot_rank = jnp.sum(jnp.cumsum(member, axis=0) * member, axis=1) - 1
    target = chosen * capacity + slot_rank
    placing = (jnp.arange(slot_total, dtype=jnp.int32)[:, None] == target[None, :]).astype(
        jnp.bfloat16
    )
    send_rows = jnp.dot(placing, normed, preferred_element_type=jnp.float32).astype(jnp.bfloat16)
    send_weights = jnp.dot(placing, route_weight, preferred_element_type=jnp.float32).astype(
        jnp.bfloat16
    )
    got_rows, got_weights = sent_together(
        (
            send_rows.reshape(group_total, capacity, -1),
            send_weights.reshape(group_total, capacity, -1),
        ),
        TP,
        0,
        0,
        2,
    )
    group_rows = got_rows.reshape(slot_total, -1)
    weights = got_weights.reshape(slot_total, -1)
    gathered = sent_together_2((gate_serve, up_serve, down_serve), "fs", 2, 0)
    summed = expert_rows(group_rows, weights, gathered)
    result = summed.astype(jnp.bfloat16).reshape(group_total, capacity, -1)
    returned = exchange_by_chip(result, ("tp_0", "tp_1"), (1, 0), 0, 0)
    mixed = jnp.einsum(
        "st,sd->td", placing, returned.reshape(slot_total, -1), preferred_element_type=jnp.float32
    ).astype(jnp.bfloat16)
    return (gate_serve, up_serve, down_serve, mixed)


def solution(mesh):
    torus = Mesh(mesh.devices.reshape(mesh.shape["fs"], 16, 2), ("fs", "tp_0", "tp_1"))
    placed = (
        P(FS_TP, None),
        P(TP),
        P(None, None, "fs", TP),
        P(None, None, "fs", TP),
        P(None, None, "fs", TP),
        P(FS_TP, None),
        P(FS_TP, None),
    )
    return jax.shard_map(
        per_device,
        mesh=torus,
        in_specs=placed,
        out_specs=(
            P(TP, None, "fs", None),
            P(TP, None, "fs", None),
            P(TP, None, "fs", None),
            P(FS_TP, None),
        ),
        check_vma=False,
    )
```

profile of v0, /device:TPU:2, one launch (start us, length us, event | category | flops | bytes accessed | tf_op | source)
XLA Modules:
  0.0 266.5 jit_solution(16070774180401151107)
XLA Ops:
  7.2 0.0 copy-start
  7.2 0.0 copy-start.2
  7.2 0.0 all-gather.2.cloned.1.call-start
  7.2 1.4 convert_element_type.46
  8.6 0.1 copy-done.2
  8.7 1.6 multiply_convert_fusion.1
  10.3 0.3 pad_maximum_fusion
  10.6 1.2 reshape.62
  11.8 60.2 %all_to_all.33 = bf16[32,2,6144]{2,1,0:T(2,128)(2,1)S(1)} all-to-all(bf16[32,2,6144]{2,1,0:T(2,128)(2,1)S(1)} %reshape.62), channel_id=1, replica_groups=mesh['fs'=16,'tp_0'=16,'tp_1'=2] {'tp_0','tp_1'}, dimensions={0} | all-to-all | bytes 1572864 | tf_op jit(solution)/shard_map/all_to_all | solution.py:17
  72.0 1.0 reshape.63
  73.0 1.0 copy.15
  74.0 1.3 all_to_all.25
  75.4 0.0 copy-start.6
  75.4 0.0 copy-start.1
  75.4 0.1 fusion.16
  75.5 0.0 copy-start.3
  75.5 0.0 copy-start.4
  75.5 0.0 copy-start.5
  75.5 1.0 pad_maximum_fusion.2
  76.5 0.0 all-gather.2.cloned.1.call-update
  76.5 0.0 copy-done.6
  76.5 0.1 fusion.13
  76.6 0.2 reduce_window_sum.11
  76.8 0.2 select_reduce_fusion
  77.0 0.0 copy-done
  77.0 0.1 convolution_convert_fusion.3
  77.1 0.1 copy.19
  77.3 0.0 copy-done.1
  77.3 0.2 fusion.3
  77.5 0.5 fusion
  78.0 0.0 copy-done.3
  78.0 0.0 copy-done.4
  78.1 0.0 copy-done.5
  78.1 0.1 pad_maximum_fusion.1
  78.2 62.3 %all_to_all.34 = bf16[32,8,2050]{2,1,0:T(8,128)(2,1)S(1)} all-to-all(bf16[32,8,2050]{2,1,0:T(8,128)(2,1)S(1)} %pad_maximum_fusion.1), channel_id=1, replica_groups=mesh['fs'=16,'tp_0'=16,'tp_1'=2] {'tp_0','tp_1'}, dimensions={0} | all-to-all | bytes 2099200 | tf_op jit(solution)/shard_map/all_to_all | solution.py:17
  140.5 0.3 mul.65
  140.8 0.2 copy.20
  141.0 32.4 %all-gather.2.cloned.1.call-done = bf16[3,2,512,2048]{3,2,1,0:T(8,128)(2,1)} async-done(((bf16[3,2,32,2048]{3,2,1,0:T(8,128)(2,1)}), bf16[3,2,512,2048]{3,2,1,0:T(8,128)(2,1)}) %all-gather.2.cloned.1.call-update) | async-done | bytes 12582928 | tf_op jit(solution)/shard_map/all_gather | solution.py:24
  173.4 7.8 %fusion.15 = (bf16[1,2,512,2048]{3,2,1,0:T(8,128)(2,1)S(1)}, bf16[1,2,512,2048]{3,2,1,0:T(8,128)(2,1)}, bf16[1,2,512,2048]{3,2,1,0:T(8,128)(2,1)}) fusion(bf16[3,2,512,2048]{3,2,1,0:T(8,128)(2,1)} %all-gather.2.cloned.1.call-done), kind=kLoop, calls=%fused_computation.33 | loop fusion | bytes 25165824 | tf_op jit(solution)/shard_map/split | solution.py:25
  181.2 2.3 fusion.5
  183.5 6.4 %convolution_convert_fusion.1 = bf16[256,2048]{1,0:T(8,128)(2,1)S(1)} fusion(bf16[1024,2048]{1,0:T(8,128)(2,1)} %bitcast.36, f32[256,1024]{1,0:T(8,128)S(1)} %bitcast.39, bf16[1024,2048]{1,0:T(8,128)(2,1)} %bitcast.37, f32[256,1024]{1,0:T(8,128)} %fusion.5, bf16[32,8,2050]{2,1,0:T(8,128)(2,1)S(1)} %all_to_all.34), kind=kOutput, calls=%fused_computation.1 | convolution fusion | flops 2149842944 | bytes 12582912 | tf_op jit(solution)/shard_map/dot_general | solution.py:69
  189.8 0.1 copy.17
  189.9 4.6 %all_to_all.35 = bf16[16,2,1,8,2048]{4,3,0,2,1:T(8,128)(2,1)S(1)} all-to-all(bf16[16,2,1,8,2048]{4,3,0,2,1:T(8,128)(2,1)S(1)} %copy.17), channel_id=1, replica_groups=mesh['fs'=16,'tp_0'=16,'tp_1'=2] {'tp_1'}, dimensions={1} | all-to-all | bytes 2097152 | tf_op jit(solution)/shard_map/all_to_all | solution.py:43
  194.5 0.1 copy.18
  194.6 63.9 %all_to_all.36 = bf16[16,2,1,8,2048]{4,3,1,2,0:T(8,128)(2,1)S(1)} all-to-all(bf16[16,2,1,8,2048]{4,3,1,2,0:T(8,128)(2,1)S(1)} %copy.18), channel_id=1, replica_groups=mesh['fs'=16,'tp_0'=16,'tp_1'=2] {'tp_0'}, dimensions={0} | all-to-all | bytes 2097152 | tf_op jit(solution)/shard_map/all_to_all | solution.py:43
  258.6 1.1 convolution_convert_fusion.2
  (3 shorter events, 0.0 us)
Async XLA Ops:
  7.2 69.8 %copy-start = (bf16[128,2]{0,1:T(2,128)(2,1)S(1)}, bf16[128,2]{0,1:T(2,128)(2,1)}, u32[]{:S(2)}) copy-start(bf16[128,2]{0,1:T(2,128)(2,1)} %param.13) | copy-start | bytes 1540
  7.2 1.5 copy-start.2
  7.2 166.2 %all-gather.2.cloned.1.call-start = ((), (), s32[]{:S(2)}) async-start(), calls=%async_computation.4 | async-start | bytes 13369344 | tf_op jit(solution)/shard_map/all_gather | solution.py:24
  75.4 1.2 copy-start.6
  75.4 1.9 copy-start.1
  75.5 2.6 copy-start.3
  75.5 2.6 copy-start.4
  75.5 2.6 copy-start.5
Sparse Core Ops, SparseCore 0:
  76.6 96.7 all-gather.1
where the time goes:
time: 267 us
  blocking collectives  191 us (72%)
  waiting for transfers between devices  32.4 us (12%)
  between operations  14.3 us (5%)
  local copies, waits for them, and re-layouts  13.4 us (5%)
  matrix products  10.4 us (4%)
  other arithmetic  5.03 us (2%)
    all_to_all x2, blocking collectives, sent_together(): lax.all_to_all(both, axis, split_axis=split_dim, concat_axis=concat_dim,...  122 us
    all_to_all x2, blocking collectives, moved_by_axis(): out = lax.all_to_all(out, axes[k], k, k, tiled=True)  68.5 us
    all_gather x1, waiting for transfers between devices, sent_together_2(): out = lax.all_gather(both, axis, axis=dim, tiled=True)  32.4 us
    split x1, local copies, waits for them, and re-layouts, sent_together_2(): jnp.split(out, [sum(widths[:k]) for k in range(1, len(widths))], axis=along)  7.79 us
    dot_general x1, matrix products, expert_rows(): return jnp.dot(hidden, down_matrix, preferred_element_type=jnp.float32)  6.36 us
  transfers between devices with their start and end apart: 1, of which 1 were waited for; matrix products, arithmetic and copies ran while one was open for 1% of the time, Pallas kernels for 0%

commit v1 on v0

v1 whole, which is shorter than its diff:
```python
import functools

import jax
import jax.numpy as jnp
from jax import lax
from jax.experimental import pallas as pl
from jax.experimental.pallas import tpu as pltpu
from jax.sharding import Mesh
from jax.sharding import PartitionSpec as P

FS = ("y", "x")
TP = ("z", "c")
ALL = ("y", "x", "z", "c")
EPS = 1e-06
MESH = pl.DeviceIdType.MESH
BF = jnp.bfloat16
F32 = jnp.float32

NY, NX, NZ = 4, 4, 16
NT = 2 * NZ
CAP = 8
TOK = 128
D = 2048
LAG1, LAG2, LAG3 = 2, 4, 6
NB = 4


def near(k):
    return ((k + 1) // 2) * (2 * (k % 2) - 1)


def far(i):
    return (8 - (i + 1) // 2) * (2 * (i % 2) - 1)


def body(
    prompt, aux, gain, gate, up, down,
    gs_out, us_out, ds_out, mixed,
    weights, wsend, pxs, pxr, xs, xr, ws, wr, hr, rr, xc, wc, acc, pt,
    px_s, px_r, w_s, w_r, g_s, g_r, x_s, x_r, a_s, a_r, r_s, r_r, o_s,
):
    y, x, z, c = (lax.axis_index(a) for a in ALL)
    me = 2 * z + c
    fs = y * NX + x
    masters = (gate, up, down)

    barrier = pltpu.get_barrier_semaphore()

    @pl.loop(1, NZ)
    def _(k):
        for cc in range(2):
            pl.semaphore_signal(
                barrier, inc=1, device_id={"z": lax.rem(z + k, NZ), "c": cc}, device_id_type=MESH
            )

    for axis, pos, n in (("x", x, NX), ("y", y, NY)):
        for step in (1, n - 1):
            pl.semaphore_signal(
                barrier, inc=1, device_id={axis: lax.rem(pos + step, n)}, device_id_type=MESH
            )
    pl.semaphore_signal(barrier, inc=1, device_id={"c": 1 - c}, device_id_type=MESH)

    gains = gain[...]

    def rounded(a, g):
        value = masters[a][g].reshape(64, 64)
        if a < 2:
            value = value * gains
        return value.astype(BF)

    @pl.loop(0, NZ)
    def _(t):
        for a in range(3):
            pxs[t, a] = rounded(a, 2 * t + 1 - c)

    pl.semaphore_wait(barrier, 2 * (NZ - 1) + 5)
    px = pltpu.make_async_remote_copy(
        src_ref=pxs, dst_ref=pxr, send_sem=px_s, recv_sem=px_r,
        device_id={"c": 1 - c}, device_id_type=MESH,
    )
    px.start()

    values = prompt[...].astype(F32)
    scale = lax.rsqrt(jnp.mean(values * values, axis=1, keepdims=True) + EPS)
    normed = (values * scale).astype(BF)
    rows = lax.broadcasted_iota(jnp.int32, (TOK, TOK), 0)
    cols = lax.broadcasted_iota(jnp.int32, (TOK, TOK), 1)

    def column(row):
        return jnp.sum(jnp.where(rows == cols, row, 0.0), axis=1, keepdims=True)

    pick_row = aux[0:1, :]
    pick_col = column(pick_row)
    same = pick_col == pick_row
    rank_row = jnp.sum(jnp.where(same & (rows < cols), 1.0, 0.0), axis=0, keepdims=True)
    rank_col = jnp.sum(jnp.where(same & (cols < rows), 1.0, 0.0), axis=1, keepdims=True)
    target_row = (pick_row * CAP + rank_row).astype(jnp.int32)
    target_col = (pick_col * CAP + rank_col).astype(jnp.int32)
    slots = lax.broadcasted_iota(jnp.int32, (TOK, NT * CAP), 1)
    pt[...] = (slots == target_col).astype(F32).astype(BF)
    for q in range(4):
        ids = lax.broadcasted_iota(jnp.int32, (64, TOK), 0) + 64 * q
        place = (ids == target_row).astype(F32).astype(BF)
        placed = jnp.dot(place, normed, preferred_element_type=F32)
        xs[8 * q : 8 * q + 8] = placed.reshape(8, CAP, D).astype(BF)
    slot_of = (cols % CAP).astype(F32)
    spread = jnp.where(cols < CAP, column(aux[1:2, :]), column(aux[2:3, :]))
    spread = jnp.where((cols < 2 * CAP) & (rank_col == slot_of), spread, 0.0).astype(BF)
    groups = lax.broadcasted_iota(jnp.int32, (NT, TOK), 0).astype(F32)
    member = (groups == pick_row).astype(F32).astype(BF)
    sent_weights = jnp.dot(member, spread, preferred_element_type=F32)
    for g in range(NT):
        ws[g] = sent_weights[g : g + 1, :]

    px.wait()
    r64 = lax.broadcasted_iota(jnp.int32, (64, 128), 0)
    c64 = lax.broadcasted_iota(jnp.int32, (64, 128), 1)
    own_half = (c64 == r64 + 64 * c).astype(F32).astype(BF)
    other_half = (c64 == r64 + 64 * (1 - c)).astype(F32).astype(BF)
    my_cols = pl.ds(pl.multiple_of(z * 128, 128), 128)

    def weight_copy(t):
        return pltpu.make_async_remote_copy(
            src_ref=wsend.at[t], dst_ref=weights.at[fs, :, :, my_cols],
            send_sem=w_s.at[t], recv_sem=w_r.at[z],
            device_id={"z": t}, device_id_type=MESH,
        )

    def join(t):
        for a in range(3):
            both = jnp.dot(rounded(a, 2 * t + c), own_half, preferred_element_type=F32) + jnp.dot(
                pxr[t, a], other_half, preferred_element_type=F32
            )
            wsend[t, a] = both.astype(BF)

    join(z)
    own_copy = pltpu.make_async_copy(
        wsend.at[z], weights.at[fs, :, :, my_cols], w_r.at[z]
    )
    own_copy.start()

    @pl.loop(1, NZ)
    def _(k):
        t = lax.rem(z + near(k) + NZ, NZ)
        join(t)
        weight_copy(t).start()

    def token_copy(tz, tc):
        t = 2 * tz + tc
        return pltpu.make_async_remote_copy(
            src_ref=xs.at[t], dst_ref=xr.at[me], send_sem=x_s.at[t], recv_sem=x_r.at[me],
            device_id={"z": tz, "c": tc}, device_id_type=MESH,
        )

    def token_weight_copy(tz, tc):
        t = 2 * tz + tc
        return pltpu.make_async_remote_copy(
            src_ref=ws.at[t], dst_ref=wr.at[me], send_sem=a_s.at[t], recv_sem=a_r.at[me],
            device_id={"z": tz, "c": tc}, device_id_type=MESH,
        )

    @pl.loop(0, NZ - 1)
    def _(i):
        tz = lax.rem(z + far(i) + NZ, NZ)
        for tc in range(2):
            token_weight_copy(tz, tc).start()
            token_copy(tz, tc).start()

    token_weight_copy(z, 1 - c).start()
    token_copy(z, 1 - c).start()
    xr[me] = xs[me]
    wr[me] = ws[me]

    def geometry(k):
        along_x = 1 - k % 2
        return along_x, 1 - along_x

    def block(k, da, db):
        ax, ay = geometry(k)
        dx = da * ax + db * ay
        dy = da * ay + db * ax
        return lax.rem(y + dy + NY, NY) * NX + lax.rem(x + dx + NX, NX)

    def piece(k, f):
        col = lax.rem(z + near(k) + NZ, NZ) * 128
        return weights.at[f, :, :, pl.ds(pl.multiple_of(col, 128), 128)]

    def push(k, f, ta, tb):
        ax, ay = geometry(k)
        tx = lax.rem(x + ta * ax + tb * ay + NX, NX)
        ty = lax.rem(y + ta * ay + tb * ax + NY, NY)
        ref = piece(k, f)
        pltpu.make_async_remote_copy(
            src_ref=ref, dst_ref=ref, send_sem=g_s, recv_sem=g_r.at[k, f],
            device_id={"y": ty, "x": tx}, device_id_type=MESH,
        ).start()

    def arrived(k, f):
        ref = piece(k, f)
        pltpu.make_async_copy(ref, ref, g_r.at[k, f]).wait()

    def turn(k):
        return 1 - 2 * ((k // 2) % 2)

    def turn_of(k, da):
        ax, ay = geometry(k)
        a = ax * x + ay * y
        return 1 - 2 * ((a + da + 4 + k // 2) % 2)

    def relay(k, da):
        s = turn_of(k, da)
        f = block(k, da, -s)
        arrived(k, f)
        push(k, f, 0, s)

    def across(k, da):
        f = block(k, da, 0)
        push(k, f, 0, 1)
        push(k, f, 0, -1)

    def stage0(k):
        src = lax.rem(z + near(k) + NZ, NZ)
        pltpu.make_async_copy(piece(k, fs), piece(k, fs), w_r.at[src]).wait()
        push(k, fs, 1, 0)
        push(k, fs, -1, 0)
        across(k, 0)

    def stage1(k):
        s = turn(k)
        f = block(k, -s, 0)
        arrived(k, f)
        push(k, f, s, 0)
        across(k, -s)
        arrived(k, block(k, s, 0))
        across(k, s)
        relay(k, 0)

    def stage2(k):
        arrived(k, block(k, 2, 0))
        across(k, 2)
        relay(k, 1)
        relay(k, -1)

    def stage3(k):
        relay(k, 2)

    @pl.loop(0, NZ + LAG3)
    def _(step):
        pl.when(step < NZ)(lambda: stage0(step))
        pl.when((step >= LAG1) & (step < NZ + LAG1))(lambda: stage1(step - LAG1))
        pl.when((step >= LAG2) & (step < NZ + LAG2))(lambda: stage2(step - LAG2))
        pl.when(step >= LAG3)(lambda: stage3(step - LAG3))

    outs = [
        pltpu.make_async_copy(weights.at[fs, a], out, o_s.at[a])
        for a, out in enumerate((gs_out, us_out, ds_out))
    ]
    for out in outs:
        out.start()

    @pl.loop(0, NZ)
    def _(k):
        for da in (0, 1, -1, 2):
            s = turn_of(k, da)
            arrived(k, block(k, da, s))
            arrived(k, block(k, da, 2))

    lane = lax.broadcasted_iota(jnp.int32, (16, 128), 1)
    row = lax.broadcasted_iota(jnp.int32, (16, 128), 0)
    BZ = NZ // NB
    M = BZ * 16

    @pl.loop(0, NB)
    def _(b):
        @pl.loop(0, BZ)
        def _(j):
            i = b * BZ + j
            sz = lax.rem(z + far(i) + NZ, NZ)
            for sc in range(2):
                t = 2 * sz + sc

                @pl.when((i < NZ - 1) | (c != sc))
                def _():
                    pltpu.make_async_copy(xs.at[t], xr.at[t], x_r.at[t]).wait()
                    pltpu.make_async_copy(ws.at[t], wr.at[t], a_r.at[t]).wait()

            at = pl.ds(pl.multiple_of(j * 16, 16), 16)
            xc[at, :] = xr[pl.ds(2 * sz, 2)].astype(F32).reshape(16, D).astype(BF)
            both = jnp.broadcast_to(wr[pl.ds(2 * sz, 2)], (2, 8, 128)).reshape(16, 128)
            w0 = jnp.sum(jnp.where(lane == row % CAP, both, 0.0), axis=1, keepdims=True)
            w1 = jnp.sum(jnp.where(lane == row % CAP + CAP, both, 0.0), axis=1, keepdims=True)
            wc[at, :] = jnp.where((lane // 32) % 2 == 0, w0, w1)

        acc[...] = jnp.zeros_like(acc)

        @pl.loop(0, 4)
        def _(q):
            part = pl.ds(4 * q, 4)
            nt = (((1,), (1,)), ((), ()))
            xx = xc[...]
            g = lax.dot_general(
                xx, weights[part, 0].reshape(256, D), nt, preferred_element_type=F32
            )
            u = lax.dot_general(
                xx, weights[part, 1].reshape(256, D), nt, preferred_element_type=F32
            )
            w = jnp.concatenate([wc[...], wc[...]], axis=1)
            h = (w * (g / (1.0 + jnp.exp(-g)) * u)).astype(BF)
            acc[...] += jnp.dot(h, weights[part, 2].reshape(256, D), preferred_element_type=F32)

        @pl.loop(0, BZ)
        def _(j):
            i = b * BZ + j
            sz = lax.rem(z + far(i) + NZ, NZ)
            at = pl.ds(pl.multiple_of(j * 16, 16), 16)
            hr[pl.ds(2 * sz, 2)] = acc[at, :].reshape(2, CAP, D).astype(BF)
            for sc in range(2):

                @pl.when((i < NZ - 1) | (c != sc))
                def _():
                    t = 2 * sz + sc
                    pltpu.make_async_remote_copy(
                        src_ref=hr.at[t], dst_ref=rr.at[me], send_sem=r_s.at[t],
                        recv_sem=r_r.at[me], device_id={"z": sz, "c": sc}, device_id_type=MESH,
                    ).start()

    rr[me] = hr[me]

    @pl.loop(1, NT)
    def _(k):
        t = lax.rem(me + k, NT)
        pltpu.make_async_copy(xs.at[t], xr.at[t], x_s.at[t]).wait()
        pltpu.make_async_copy(ws.at[t], wr.at[t], a_s.at[t]).wait()

    @pl.loop(1, NZ)
    def _(k):
        t = lax.rem(z + k, NZ)
        pltpu.make_async_copy(wsend.at[t], wsend.at[t], w_s.at[t]).wait()

    sent = weights.at[pl.ds(0, 15)]
    pltpu.make_async_copy(sent, sent, g_s).wait()
    for out in outs:
        out.wait()

    @pl.loop(1, NT)
    def _(k):
        t = lax.rem(me + k, NT)
        pltpu.make_async_copy(hr.at[t], rr.at[t], r_r.at[t]).wait()
        pltpu.make_async_copy(hr.at[t], rr.at[t], r_s.at[t]).wait()

    for q in range(4):
        cut = slice(512 * q, 512 * q + 512)
        back = rr[:, :, cut].astype(F32).reshape(NT * CAP, 512).astype(BF)
        mixed[:, cut] = jnp.dot(pt[...], back, preferred_element_type=F32).astype(BF)


def per_device(prompt, norm_gain, gate_master, up_master, down_master, group_pick, route_weight):
    aux = jnp.concatenate(
        [
            group_pick.astype(F32).T,
            route_weight.astype(F32).T,
            jnp.zeros((5, TOK), F32),
        ],
        axis=0,
    )
    dma = pltpu.SemaphoreType.DMA
    vmem = pl.BlockSpec(memory_space=pltpu.VMEM)
    hbm = pl.BlockSpec(memory_space=pl.ANY)
    serve = jax.ShapeDtypeStruct((2 * 32, D), BF)
    gs, us, ds, mixed = pl.pallas_call(
        body,
        name="relay",
        out_shape=(serve, serve, serve, jax.ShapeDtypeStruct((TOK, D), BF)),
        in_specs=[vmem] * 6,
        out_specs=(hbm, hbm, hbm, vmem),
        scratch_shapes=[
            pltpu.VMEM((16, 3, 64, D), BF),
            pltpu.VMEM((NZ, 3, 64, 128), BF),
            pltpu.VMEM((NZ, 3, 64, 64), BF),
            pltpu.VMEM((NZ, 3, 64, 64), BF),
            pltpu.VMEM((NT, CAP, D), BF),
            pltpu.VMEM((NT, CAP, D), BF),
            pltpu.VMEM((NT, 1, 128), F32),
            pltpu.VMEM((NT, 1, 128), F32),
            pltpu.VMEM((NT, CAP, D), BF),
            pltpu.VMEM((NT, CAP, D), BF),
            pltpu.VMEM((256 // NB, D), BF),
            pltpu.VMEM((256 // NB, 128), F32),
            pltpu.VMEM((256 // NB, D), F32),
            pltpu.VMEM((TOK, NT * CAP), BF),
            dma, dma,
            dma((NZ,)), dma((NZ,)),
            dma, dma((NZ, 16)),
            dma((NT,)), dma((NT,)),
            dma((NT,)), dma((NT,)),
            dma((NT,)), dma((NT,)),
            dma((3,)),
        ],
        compiler_params=pltpu.CompilerParams(
            collective_id=0, has_side_effects=True, vmem_limit_bytes=56 * 1024 * 1024
        ),
    )(prompt, aux, norm_gain.reshape(1, 64), gate_master, up_master, down_master)
    shape = (1, 2, 32, D)
    return gs.reshape(shape), us.reshape(shape), ds.reshape(shape), mixed


def solution(mesh):
    torus = Mesh(mesh.devices.reshape(NY, NX, NZ, 2), ALL)
    placed = (
        P(ALL, None),
        P(TP),
        P(None, None, FS, TP),
        P(None, None, FS, TP),
        P(None, None, FS, TP),
        P(ALL, None),
        P(ALL, None),
    )
    serve = P(TP, None, FS, None)
    return jax.shard_map(
        per_device,
        mesh=torus,
        in_specs=placed,
        out_specs=(serve, serve, serve, P(ALL, None)),
        check_vma=False,
    )
```

time: 267 us -> 159 us (0.60)
  the two profiles are of different devices: /device:TPU:2 before, /device:TPU:1 now
where the time goes in v1:
time: 159 us
  Pallas kernels  152 us (96%)
  local copies, waits for them, and re-layouts  5.24 us (3%)
    pallas_call x1, Pallas kernels, per_device(): pl.pallas_call(body, name='relay', out_shape=(serve, serve, serve, jax.Sh...  152 us
    unnamed x14, local copies, waits for them, and re-layouts  5.16 us

profile of v1, /device:TPU:1, one launch (start us, length us, event | category | flops | bytes accessed | tf_op | source)
XLA Modules:
  0.0 158.7 jit_solution(11376875193158371999)
XLA Ops:
  0.6 0.0 copy-start.3
  0.6 0.6 copy-done.3
  1.3 0.0 copy-start.4
  1.3 0.1 pad.2.clone
  1.4 0.6 copy-done.4
  2.0 0.7 maximum_maximum_fusion.aux
  2.6 152.1 %relay.1 = (bf16[64,2048]{1,0:T(8,128)(2,1)}, bf16[64,2048]{1,0:T(8,128)(2,1)}, bf16[64,2048]{1,0:T(8,128)(2,1)}, bf16[128,2048]{1,0:T(8,128)(2,1)}) custom-call(bf16[128,2048]{1,0:T(8,128)(2,1)} %prompt.1, f32[8,128]{1,0:T(8,128)} %maximum_maximum_fusion.aux, f32[1,64]{1,0:T(1,128)} %bitcast.11, f32[32,2,32,64]{3,2,1,0:T(8,128)} %gate.1, ...), custom_call_target="tpu_custom_call" | custom-call | tf_op jit(solution)/shard_map/relay/pallas_call | solution.py:370
  154.7 0.0 copy-start.2
  154.8 0.0 copy-start.1
  154.8 1.7 %copy.15 = bf16[1,2,32,2048]{3,2,1,0:T(8,128)(2,1)} copy(bf16[1,2,32,2048]{3,2,1,0:T(8,128)(2,1)} %bitcast.10) | data formatting | bytes 524288
  156.5 0.0 copy-done.2
  156.5 0.0 copy-start
  156.5 0.7 copy.16
  157.2 0.0 copy-done.1
  157.2 0.7 copy.17
  157.9 0.0 copy-done
  157.9 0.8 copy.18
  (3 shorter events, 0.0 us)
Async XLA Ops:
  0.6 0.7 copy-start.3
  1.3 0.7 copy-start.4
  154.7 1.7 %copy-start.2 = (bf16[64,2048]{1,0:T(8,128)(2,1)S(1)}, bf16[64,2048]{1,0:T(8,128)(2,1)}, u32[]{:S(2)}) copy-start(bf16[64,2048]{1,0:T(8,128)(2,1)} %get-tuple-element.9) | copy-start | bytes 786436
  154.8 2.4 %copy-start.1 = (bf16[64,2048]{1,0:T(8,128)(2,1)S(1)}, bf16[64,2048]{1,0:T(8,128)(2,1)}, u32[]{:S(2)}) copy-start(bf16[64,2048]{1,0:T(8,128)(2,1)} %get-tuple-element.10) | copy-start | bytes 786436
  156.5 1.4 copy-start

commit v2 on v1

--- a/solution.py
+++ b/solution.py
@@ -22,6 +22,7 @@
 TOK = 128
 D = 2048
 LAG1, LAG2, LAG3 = 2, 4, 6
+FIRST = 1
 NB = 4
 
 
@@ -34,10 +35,11 @@
 
 
 def body(
-    prompt, aux, gain, gate, up, down,
+    prompt_hbm, pick, route, gain, gate_hbm, up_hbm, down_hbm,
     gs_out, us_out, ds_out, mixed,
+    prompt, gate, up, down,
     weights, wsend, pxs, pxr, xs, xr, ws, wr, hr, rr, xc, wc, acc, pt,
-    px_s, px_r, w_s, w_r, g_s, g_r, x_s, x_r, a_s, a_r, r_s, r_r, o_s,
+    px_s, px_r, w_s, w_r, g_s, g_r, x_s, x_r, a_s, a_r, r_s, r_r, o_s, i_s,
 ):
     y, x, z, c = (lax.axis_index(a) for a in ALL)
     me = 2 * z + c
@@ -46,12 +48,11 @@
 
     barrier = pltpu.get_barrier_semaphore()
 
-    @pl.loop(1, NZ)
-    def _(k):
+    @pl.loop(0, NZ - 1)
+    def _(i):
+        tz = lax.rem(z + far(i) + NZ, NZ)
         for cc in range(2):
-            pl.semaphore_signal(
-                barrier, inc=1, device_id={"z": lax.rem(z + k, NZ), "c": cc}, device_id_type=MESH
-            )
+            pl.semaphore_signal(barrier, inc=1, device_id={"z": tz, "c": cc}, device_id_type=MESH)
 
     for axis, pos, n in (("x", x, NX), ("y", y, NY)):
         for step in (1, n - 1):
@@ -60,6 +61,15 @@
             )
     pl.semaphore_signal(barrier, inc=1, device_id={"c": 1 - c}, device_id_type=MESH)
 
+    loads = [
+        pltpu.make_async_copy(src, dst, i_s.at[n])
+        for n, (src, dst) in enumerate(
+            ((prompt_hbm, prompt), (gate_hbm, gate), (up_hbm, up), (down_hbm, down))
+        )
+    ]
+    for load in loads:
+        load.start()
+
     gains = gain[...]
 
     def rounded(a, g):
@@ -68,18 +78,15 @@
             value = value * gains
         return value.astype(BF)
 
+    for load in loads[1:]:
+        load.wait()
+
     @pl.loop(0, NZ)
     def _(t):
         for a in range(3):
             pxs[t, a] = rounded(a, 2 * t + 1 - c)
 
-    pl.semaphore_wait(barrier, 2 * (NZ - 1) + 5)
-    px = pltpu.make_async_remote_copy(
-        src_ref=pxs, dst_ref=pxr, send_sem=px_s, recv_sem=px_r,
-        device_id={"c": 1 - c}, device_id_type=MESH,
-    )
-    px.start()
-
+    loads[0].wait()
     values = prompt[...].astype(F32)
     scale = lax.rsqrt(jnp.mean(values * values, axis=1, keepdims=True) + EPS)
     normed = (values * scale).astype(BF)
@@ -89,7 +96,8 @@
     def column(row):
         return jnp.sum(jnp.where(rows == cols, row, 0.0), axis=1, keepdims=True)
 
-    pick_row = aux[0:1, :]
+    pick_row = pick[...].astype(F32)
+    routes = route[...].astype(F32)
     pick_col = column(pick_row)
     same = pick_col == pick_row
     rank_row = jnp.sum(jnp.where(same & (rows < cols), 1.0, 0.0), axis=0, keepdims=True)
@@ -104,7 +112,7 @@
         placed = jnp.dot(place, normed, preferred_element_type=F32)
         xs[8 * q : 8 * q + 8] = placed.reshape(8, CAP, D).astype(BF)
     slot_of = (cols % CAP).astype(F32)
-    spread = jnp.where(cols < CAP, column(aux[1:2, :]), column(aux[2:3, :]))
+    spread = jnp.where(cols < CAP, column(routes[0:1, :]), column(routes[1:2, :]))
     spread = jnp.where((cols < 2 * CAP) & (rank_col == slot_of), spread, 0.0).astype(BF)
     groups = lax.broadcasted_iota(jnp.int32, (NT, TOK), 0).astype(F32)
     member = (groups == pick_row).astype(F32).astype(BF)
@@ -112,6 +120,34 @@
     for g in range(NT):
         ws[g] = sent_weights[g : g + 1, :]
 
+    pl.semaphore_wait(barrier, 2 * (NZ - 1) + 5)
+    px = pltpu.make_async_remote_copy(
+        src_ref=pxs, dst_ref=pxr, send_sem=px_s, recv_sem=px_r,
+        device_id={"c": 1 - c}, device_id_type=MESH,
+    )
+    px.start()
+
+    def token_copy(tz, tc):
+        t = 2 * tz + tc
+        return pltpu.make_async_remote_copy(
+            src_ref=xs.at[t], dst_ref=xr.at[me], send_sem=x_s.at[t], recv_sem=x_r.at[me],
+            device_id={"z": tz, "c": tc}, device_id_type=MESH,
+        )
+
+    def token_weight_copy(tz, tc):
+        t = 2 * tz + tc
+        return pltpu.make_async_remote_copy(
+            src_ref=ws.at[t], dst_ref=wr.at[me], send_sem=a_s.at[t], recv_sem=a_r.at[me],
+            device_id={"z": tz, "c": tc}, device_id_type=MESH,
+        )
+
+    @pl.loop(0, FIRST)
+    def _(i):
+        tz = lax.rem(z + far(i) + NZ, NZ)
+        for tc in range(2):
+            token_weight_copy(tz, tc).start()
+            token_copy(tz, tc).start()
+
     px.wait()
     r64 = lax.broadcasted_iota(jnp.int32, (64, 128), 0)
     c64 = lax.broadcasted_iota(jnp.int32, (64, 128), 1)
@@ -145,21 +181,7 @@
         join(t)
         weight_copy(t).start()
 
-    def token_copy(tz, tc):
-        t = 2 * tz + tc
-        return pltpu.make_async_remote_copy(
-            src_ref=xs.at[t], dst_ref=xr.at[me], send_sem=x_s.at[t], recv_sem=x_r.at[me],
-            device_id={"z": tz, "c": tc}, device_id_type=MESH,
-        )
-
-    def token_weight_copy(tz, tc):
-        t = 2 * tz + tc
-        return pltpu.make_async_remote_copy(
-            src_ref=ws.at[t], dst_ref=wr.at[me], send_sem=a_s.at[t], recv_sem=a_r.at[me],
-            device_id={"z": tz, "c": tc}, device_id_type=MESH,
-        )
-
-    @pl.loop(0, NZ - 1)
+    @pl.loop(FIRST, NZ - 1)
     def _(i):
         tz = lax.rem(z + far(i) + NZ, NZ)
         for tc in range(2):
@@ -354,26 +376,29 @@
         mixed[:, cut] = jnp.dot(pt[...], back, preferred_element_type=F32).astype(BF)
 
 
+def written(*refs):
+    sems = refs[8]
+    copies = [pltpu.make_async_copy(refs[n], refs[4 + n], sems.at[n]) for n in range(4)]
+    for copy in copies:
+        copy.start()
+    for copy in copies:
+        copy.wait()
+
+
 def per_device(prompt, norm_gain, gate_master, up_master, down_master, group_pick, route_weight):
-    aux = jnp.concatenate(
-        [
-            group_pick.astype(F32).T,
-            route_weight.astype(F32).T,
-            jnp.zeros((5, TOK), F32),
-        ],
-        axis=0,
-    )
     dma = pltpu.SemaphoreType.DMA
     vmem = pl.BlockSpec(memory_space=pltpu.VMEM)
     hbm = pl.BlockSpec(memory_space=pl.ANY)
-    serve = jax.ShapeDtypeStruct((2 * 32, D), BF)
+    serve = pltpu.VMEM((2 * 32, D), BF)
     gs, us, ds, mixed = pl.pallas_call(
         body,
         name="relay",
-        out_shape=(serve, serve, serve, jax.ShapeDtypeStruct((TOK, D), BF)),
-        in_specs=[vmem] * 6,
-        out_specs=(hbm, hbm, hbm, vmem),
+        out_shape=(serve, serve, serve, pltpu.VMEM((TOK, D), BF)),
+        in_specs=[hbm] + [vmem] * 3 + [hbm] * 3,
+        out_specs=(vmem,) * 4,
         scratch_shapes=[
+            pltpu.VMEM((TOK, D), BF),
+            *[pltpu.VMEM((32, 2, 32, 64), F32)] * 3,
             pltpu.VMEM((16, 3, 64, D), BF),
             pltpu.VMEM((NZ, 3, 64, 128), BF),
             pltpu.VMEM((NZ, 3, 64, 64), BF),
@@ -395,11 +420,20 @@
             dma((NT,)), dma((NT,)),
             dma((NT,)), dma((NT,)),
             dma((3,)),
+            dma((4,)),
         ],
         compiler_params=pltpu.CompilerParams(
             collective_id=0, has_side_effects=True, vmem_limit_bytes=56 * 1024 * 1024
         ),
-    )(prompt, aux, norm_gain.reshape(1, 64), gate_master, up_master, down_master)
+    )(prompt, group_pick.T, route_weight.T, norm_gain.reshape(1, 64), gate_master, up_master, down_master)
+    gs, us, ds, mixed = pl.pallas_call(
+        written,
+        name="written",
+        out_shape=tuple(jax.ShapeDtypeStruct(a.shape, BF) for a in (gs, us, ds, mixed)),
+        in_specs=[vmem] * 4,
+        out_specs=(hbm,) * 4,
+        scratch_shapes=[dma((4,))],
+    )(*(pltpu.with_memory_space_constraint(a, pltpu.VMEM) for a in (gs, us, ds, mixed)))
     shape = (1, 2, 32, D)
     return gs.reshape(shape), us.reshape(shape), ds.reshape(shape), mixed
 

time: 159 us -> 152 us (0.956)
  local copies, waits for them, and re-layouts: 5.24 us -> 0 us
    unnamed x14 -> x0, local copies, waits for them, and re-layouts: 5.16 us -> none
    pallas_call x1 -> x2, Pallas kernels: 152 us -> 151 us  [the longest x1 150 us: per_device(): pl.pallas_call(body, name='relay', out_shape=(serve, serve, serve, pltpu....]
where the time goes in v2:
time: 152 us
  Pallas kernels  151 us (99%)
    pallas_call x1, Pallas kernels, per_device(): pl.pallas_call(body, name='relay', out_shape=(serve, serve, serve, pltpu....  150 us

profile of v2, /device:TPU:1, one launch (start us, length us, event | category | flops | bytes accessed | tf_op | source)
XLA Modules:
  0.0 151.8 jit_solution(6262100481532705772)
XLA Ops:
  0.6 150.1 %relay.1 = (bf16[64,2048]{1,0:T(8,128)(2,1)S(1)}, bf16[64,2048]{1,0:T(8,128)(2,1)S(1)}, bf16[64,2048]{1,0:T(8,128)(2,1)S(1)}, bf16[128,2048]{1,0:T(8,128)(2,1)S(1)}) custom-call(bf16[128,2048]{1,0:T(8,128)(2,1)} %prompt_hbm.1, s32[1,128]{1,0:T(1,128)} %bitcast.6, bf16[2,128]{1,0:T(2,128)(2,1)} %bitcast.7, f32[1,64]{1,0:T(1,128)} %bitcast.8, ...), custom_call_target="tpu_custom_call" | custom-call | tf_op jit(solution)/shard_map/relay/pallas_call | solution.py:393
  150.7 1.1 written.1

commit v3 on v2

--- a/solution.py
+++ b/solution.py
@@ -22,7 +22,7 @@
 TOK = 128
 D = 2048
 LAG1, LAG2, LAG3 = 2, 4, 6
-FIRST = 1
+EARLY = 3
 NB = 4
 
 
@@ -39,7 +39,7 @@
     gs_out, us_out, ds_out, mixed,
     prompt, gate, up, down,
     weights, wsend, pxs, pxr, xs, xr, ws, wr, hr, rr, xc, wc, acc, pt,
-    px_s, px_r, w_s, w_r, g_s, g_r, x_s, x_r, a_s, a_r, r_s, r_r, o_s, i_s,
+    px_s, px_r, w_s, w_r, g_s, g_r, x_s, x_r, a_s, a_r, r_s, r_r, o_s, i_s, chain, normed,
 ):
     y, x, z, c = (lax.axis_index(a) for a in ALL)
     me = 2 * z + c
@@ -48,13 +48,7 @@
 
     barrier = pltpu.get_barrier_semaphore()
 
-    @pl.loop(0, NZ - 1)
-    def _(i):
-        tz = lax.rem(z + far(i) + NZ, NZ)
-        for cc in range(2):
-            pl.semaphore_signal(barrier, inc=1, device_id={"z": tz, "c": cc}, device_id_type=MESH)
-
-    for axis, pos, n in (("x", x, NX), ("y", y, NY)):
+    for axis, pos, n in (("z", z, NZ), ("x", x, NX), ("y", y, NY)):
         for step in (1, n - 1):
             pl.semaphore_signal(
                 barrier, inc=1, device_id={axis: lax.rem(pos + step, n)}, device_id_type=MESH
@@ -86,10 +80,31 @@
         for a in range(3):
             pxs[t, a] = rounded(a, 2 * t + 1 - c)
 
+    pl.semaphore_wait(barrier, 7)
+
+    def tell(j):
+        pl.semaphore_signal(
+            chain.at[0, j], inc=1, device_id={"z": lax.rem(z + 1, NZ)}, device_id_type=MESH
+        )
+        pl.semaphore_signal(
+            chain.at[1, j], inc=1, device_id={"z": lax.rem(z + NZ - 1, NZ)}, device_id_type=MESH
+        )
+
+    def hear(j):
+        pl.semaphore_wait(chain.at[0, j], 1)
+        pl.semaphore_wait(chain.at[1, j], 1)
+
+    tell(1)
+    px = pltpu.make_async_remote_copy(
+        src_ref=pxs, dst_ref=pxr, send_sem=px_s, recv_sem=px_r,
+        device_id={"c": 1 - c}, device_id_type=MESH,
+    )
+    px.start()
+
     loads[0].wait()
     values = prompt[...].astype(F32)
     scale = lax.rsqrt(jnp.mean(values * values, axis=1, keepdims=True) + EPS)
-    normed = (values * scale).astype(BF)
+    normed[...] = (values * scale).astype(BF)
     rows = lax.broadcasted_iota(jnp.int32, (TOK, TOK), 0)
     cols = lax.broadcasted_iota(jnp.int32, (TOK, TOK), 1)
 
@@ -106,10 +121,159 @@
     target_col = (pick_col * CAP + rank_col).astype(jnp.int32)
     slots = lax.broadcasted_iota(jnp.int32, (TOK, NT * CAP), 1)
     pt[...] = (slots == target_col).astype(F32).astype(BF)
+    hear(1)
+    tell(2)
+
+    r64 = lax.broadcasted_iota(jnp.int32, (64, 128), 0)
+    c64 = lax.broadcasted_iota(jnp.int32, (64, 128), 1)
+    own_half = (c64 == r64 + 64 * c).astype(F32).astype(BF)
+    other_half = (c64 == r64 + 64 * (1 - c)).astype(F32).astype(BF)
+    my_cols = pl.ds(pl.multiple_of(z * 128, 128), 128)
+
+    def weight_copy(t):
+        return pltpu.make_async_remote_copy(
+            src_ref=wsend.at[t], dst_ref=weights.at[fs, :, :, my_cols],
+            send_sem=w_s.at[t], recv_sem=w_r.at[z],
+            device_id={"z": t}, device_id_type=MESH,
+        )
+
+    def join(t, put):
+        for a in range(3):
+            both = jnp.dot(rounded(a, 2 * t + c), own_half, preferred_element_type=F32) + jnp.dot(
+                pxr[t, a], other_half, preferred_element_type=F32
+            )
+            put(a, both.astype(BF))
+
+    def put_own(a, value):
+        weights[fs, a, :, my_cols] = value
+
+    def send_weights(t):
+        def put(a, value):
+            wsend[t, a] = value
+
+        join(t, put)
+        weight_copy(t).start()
+
+    def weights_at(j):
+        send_weights(lax.rem(z + j, NZ))
+        pl.when(j < NZ // 2)(lambda: send_weights(lax.rem(z + NZ - j, NZ)))
+
+        @pl.when(j <= 6)
+        def _():
+            hear(j + 2)
+            pl.when(j <= 5)(lambda: tell(j + 3))
+
+    def token_copy(tz, tc):
+        t = 2 * tz + tc
+        return pltpu.make_async_remote_copy(
+            src_ref=xs.at[t], dst_ref=xr.at[me], send_sem=x_s.at[t], recv_sem=x_r.at[me],
+            device_id={"z": tz, "c": tc}, device_id_type=MESH,
+        )
+
+    def token_weight_copy(tz, tc):
+        t = 2 * tz + tc
+        return pltpu.make_async_remote_copy(
+            src_ref=ws.at[t], dst_ref=wr.at[me], send_sem=a_s.at[t], recv_sem=a_r.at[me],
+            device_id={"z": tz, "c": tc}, device_id_type=MESH,
+        )
+
+    def geometry(k):
+        along_x = 1 - k % 2
+        return along_x, 1 - along_x
+
+    def block(k, da, db):
+        ax, ay = geometry(k)
+        dx = da * ax + db * ay
+        dy = da * ay + db * ax
+        return lax.rem(y + dy + NY, NY) * NX + lax.rem(x + dx + NX, NX)
+
+    def piece(k, f):
+        col = lax.rem(z + near(k) + NZ, NZ) * 128
+        return weights.at[f, :, :, pl.ds(pl.multiple_of(col, 128), 128)]
+
+    def push(k, f, ta, tb):
+        ax, ay = geometry(k)
+        tx = lax.rem(x + ta * ax + tb * ay + NX, NX)
+        ty = lax.rem(y + ta * ay + tb * ax + NY, NY)
+        ref = piece(k, f)
+        pltpu.make_async_remote_copy(
+            src_ref=ref, dst_ref=ref, send_sem=g_s, recv_sem=g_r.at[k, f],
+            device_id={"y": ty, "x": tx}, device_id_type=MESH,
+        ).start()
+
+    def arrived(k, f):
+        ref = piece(k, f)
+        pltpu.make_async_copy(ref, ref, g_r.at[k, f]).wait()
+
+    def turn(k):
+        return 1 - 2 * ((k // 2) % 2)
+
+    def turn_of(k, da):
+        ax, ay = geometry(k)
+        a = ax * x + ay * y
+        return 1 - 2 * ((a + da + 4 + k // 2) % 2)
+
+    def relay(k, da):
+        s = turn_of(k, da)
+        f = block(k, da, -s)
+        arrived(k, f)
+        push(k, f, 0, s)
+
+    def across(k, da):
+        f = block(k, da, 0)
+        push(k, f, 0, 1)
+        push(k, f, 0, -1)
+
+    def stage0(k):
+        src = lax.rem(z + near(k) + NZ, NZ)
+
+        @pl.when(k > 0)
+        def _():
+            pltpu.make_async_copy(piece(k, fs), piece(k, fs), w_r.at[src]).wait()
+
+        push(k, fs, 1, 0)
+        push(k, fs, -1, 0)
+        across(k, 0)
+
+    def stage1(k):
+        s = turn(k)
+        f = block(k, -s, 0)
+        arrived(k, f)
+        push(k, f, s, 0)
+        across(k, -s)
+        arrived(k, block(k, s, 0))
+        across(k, s)
+        relay(k, 0)
+
+    def stage2(k):
+        arrived(k, block(k, 2, 0))
+        across(k, 2)
+        relay(k, 1)
+        relay(k, -1)
+
+    def stage3(k):
+        relay(k, 2)
+
+    def stages(step):
+        pl.when(step < NZ)(lambda: stage0(step))
+        pl.when((step >= LAG1) & (step < NZ + LAG1))(lambda: stage1(step - LAG1))
+        pl.when((step >= LAG2) & (step < NZ + LAG2))(lambda: stage2(step - LAG2))
+        pl.when(step >= LAG3)(lambda: stage3(step - LAG3))
+
+    px.wait()
+    join(z, put_own)
+    stage0(0)
+    hear(2)
+    tell(3)
+
+    @pl.loop(1, EARLY + 1)
+    def _(j):
+        weights_at(j)
+
     for q in range(4):
         ids = lax.broadcasted_iota(jnp.int32, (64, TOK), 0) + 64 * q
         place = (ids == target_row).astype(F32).astype(BF)
-        placed = jnp.dot(place, normed, preferred_element_type=F32)
+        placed = jnp.dot(place, normed[...], preferred_element_type=F32)
         xs[8 * q : 8 * q + 8] = placed.reshape(8, CAP, D).astype(BF)
     slot_of = (cols % CAP).astype(F32)
     spread = jnp.where(cols < CAP, column(routes[0:1, :]), column(routes[1:2, :]))
@@ -120,158 +284,26 @@
     for g in range(NT):
         ws[g] = sent_weights[g : g + 1, :]
 
-    pl.semaphore_wait(barrier, 2 * (NZ - 1) + 5)
-    px = pltpu.make_async_remote_copy(
-        src_ref=pxs, dst_ref=pxr, send_sem=px_s, recv_sem=px_r,
-        device_id={"c": 1 - c}, device_id_type=MESH,
-    )
-    px.start()
-
-    def token_copy(tz, tc):
-        t = 2 * tz + tc
-        return pltpu.make_async_remote_copy(
-            src_ref=xs.at[t], dst_ref=xr.at[me], send_sem=x_s.at[t], recv_sem=x_r.at[me],
-            device_id={"z": tz, "c": tc}, device_id_type=MESH,
-        )
-
-    def token_weight_copy(tz, tc):
-        t = 2 * tz + tc
-        return pltpu.make_async_remote_copy(
-            src_ref=ws.at[t], dst_ref=wr.at[me], send_sem=a_s.at[t], recv_sem=a_r.at[me],
-            device_id={"z": tz, "c": tc}, device_id_type=MESH,
-        )
-
-    @pl.loop(0, FIRST)
+    @pl.loop(1, NZ // 2 - EARLY + 1)
+    def _(step):
+        weights_at(step + EARLY)
+        stages(step)
+
+    @pl.loop(0, NZ - 1)
     def _(i):
         tz = lax.rem(z + far(i) + NZ, NZ)
         for tc in range(2):
             token_weight_copy(tz, tc).start()
             token_copy(tz, tc).start()
 
-    px.wait()
-    r64 = lax.broadcasted_iota(jnp.int32, (64, 128), 0)
-    c64 = lax.broadcasted_iota(jnp.int32, (64, 128), 1)
-    own_half = (c64 == r64 + 64 * c).astype(F32).astype(BF)
-    other_half = (c64 == r64 + 64 * (1 - c)).astype(F32).astype(BF)
-    my_cols = pl.ds(pl.multiple_of(z * 128, 128), 128)
-
-    def weight_copy(t):
-        return pltpu.make_async_remote_copy(
-            src_ref=wsend.at[t], dst_ref=weights.at[fs, :, :, my_cols],
-            send_sem=w_s.at[t], recv_sem=w_r.at[z],
-            device_id={"z": t}, device_id_type=MESH,
-        )
-
-    def join(t):
-        for a in range(3):
-            both = jnp.dot(rounded(a, 2 * t + c), own_half, preferred_element_type=F32) + jnp.dot(
-                pxr[t, a], other_half, preferred_element_type=F32
-            )
-            wsend[t, a] = both.astype(BF)
-
-    join(z)
-    own_copy = pltpu.make_async_copy(
-        wsend.at[z], weights.at[fs, :, :, my_cols], w_r.at[z]
-    )
-    own_copy.start()
-
-    @pl.loop(1, NZ)
-    def _(k):
-        t = lax.rem(z + near(k) + NZ, NZ)
-        join(t)
-        weight_copy(t).start()
-
-    @pl.loop(FIRST, NZ - 1)
-    def _(i):
-        tz = lax.rem(z + far(i) + NZ, NZ)
-        for tc in range(2):
-            token_weight_copy(tz, tc).start()
-            token_copy(tz, tc).start()
-
     token_weight_copy(z, 1 - c).start()
     token_copy(z, 1 - c).start()
     xr[me] = xs[me]
     wr[me] = ws[me]
 
-    def geometry(k):
-        along_x = 1 - k % 2
-        return along_x, 1 - along_x
-
-    def block(k, da, db):
-        ax, ay = geometry(k)
-        dx = da * ax + db * ay
-        dy = da * ay + db * ax
-        return lax.rem(y + dy + NY, NY) * NX + lax.rem(x + dx + NX, NX)
-
-    def piece(k, f):
-        col = lax.rem(z + near(k) + NZ, NZ) * 128
-        return weights.at[f, :, :, pl.ds(pl.multiple_of(col, 128), 128)]
-
-    def push(k, f, ta, tb):
-        ax, ay = geometry(k)
-        tx = lax.rem(x + ta * ax + tb * ay + NX, NX)
-        ty = lax.rem(y + ta * ay + tb * ax + NY, NY)
-        ref = piece(k, f)
-        pltpu.make_async_remote_copy(
-            src_ref=ref, dst_ref=ref, send_sem=g_s, recv_sem=g_r.at[k, f],
-            device_id={"y": ty, "x": tx}, device_id_type=MESH,
-        ).start()
-
-    def arrived(k, f):
-        ref = piece(k, f)
-        pltpu.make_async_copy(ref, ref, g_r.at[k, f]).wait()
-
-    def turn(k):
-        return 1 - 2 * ((k // 2) % 2)
-
-    def turn_of(k, da):
-        ax, ay = geometry(k)
-        a = ax * x + ay * y
-        return 1 - 2 * ((a + da + 4 + k // 2) % 2)
-
-    def relay(k, da):
-        s = turn_of(k, da)
-        f = block(k, da, -s)
-        arrived(k, f)
-        push(k, f, 0, s)
-
-    def across(k, da):
-        f = block(k, da, 0)
-        push(k, f, 0, 1)
-        push(k, f, 0, -1)
-
-    def stage0(k):
-        src = lax.rem(z + near(k) + NZ, NZ)
-        pltpu.make_async_copy(piece(k, fs), piece(k, fs), w_r.at[src]).wait()
-        push(k, fs, 1, 0)
-        push(k, fs, -1, 0)
-        across(k, 0)
-
-    def stage1(k):
-        s = turn(k)
-        f = block(k, -s, 0)
-        arrived(k, f)
-        push(k, f, s, 0)
-        across(k, -s)
-        arrived(k, block(k, s, 0))
-        across(k, s)
-        relay(k, 0)
-
-    def stage2(k):
-        arrived(k, block(k, 2, 0))
-        across(k, 2)
-        relay(k, 1)
-        relay(k, -1)
-
-    def stage3(k):
-        relay(k, 2)
-
-    @pl.loop(0, NZ + LAG3)
+    @pl.loop(NZ // 2 - EARLY + 1, NZ + LAG3)
     def _(step):
-        pl.when(step < NZ)(lambda: stage0(step))
-        pl.when((step >= LAG1) & (step < NZ + LAG1))(lambda: stage1(step - LAG1))
-        pl.when((step >= LAG2) & (step < NZ + LAG2))(lambda: stage2(step - LAG2))
-        pl.when(step >= LAG3)(lambda: stage3(step - LAG3))
+        stages(step)
 
     outs = [
         pltpu.make_async_copy(weights.at[fs, a], out, o_s.at[a])
@@ -421,6 +453,8 @@
             dma((NT,)), dma((NT,)),
             dma((3,)),
             dma((4,)),
+            pltpu.SemaphoreType.REGULAR((2, NZ // 2 + 1)),
+            pltpu.VMEM((TOK, D), BF),
         ],
         compiler_params=pltpu.CompilerParams(
             collective_id=0, has_side_effects=True, vmem_limit_bytes=56 * 1024 * 1024

time: 152 us -> 150 us (0.987)
  Pallas kernels: 151 us -> 149 us
    pallas_call x1, Pallas kernels: 150 us -> 148 us  [per_device(): pl.pallas_call(body, name='relay', out_shape=(serve, serve, serve, pltpu....]
where the time goes in v3:
time: 150 us; the launch traced here: 149 us
  Pallas kernels  149 us (99%)
    pallas_call x1, Pallas kernels, per_device(): pl.pallas_call(body, name='relay', out_shape=(serve, serve, serve, pltpu....  148 us

profile of v3, /device:TPU:1, one launch (start us, length us, event | category | flops | bytes accessed | tf_op | source)
XLA Modules:
  0.0 149.5 jit_solution(15729884586223606084)
XLA Ops:
  0.6 147.8 %relay.1 = (bf16[64,2048]{1,0:T(8,128)(2,1)S(1)}, bf16[64,2048]{1,0:T(8,128)(2,1)S(1)}, bf16[64,2048]{1,0:T(8,128)(2,1)S(1)}, bf16[128,2048]{1,0:T(8,128)(2,1)S(1)}) custom-call(bf16[128,2048]{1,0:T(8,128)(2,1)} %prompt_hbm.1, s32[1,128]{1,0:T(1,128)} %bitcast.6, bf16[2,128]{1,0:T(2,128)(2,1)} %bitcast.7, f32[1,64]{1,0:T(1,128)} %bitcast.8, ...), custom_call_target="tpu_custom_call" | custom-call | tf_op jit(solution)/shard_map/relay/pallas_call | solution.py:425
  148.4 1.1 written.1

commit v4 on v3

--- a/solution.py
+++ b/solution.py
@@ -39,7 +39,7 @@
     gs_out, us_out, ds_out, mixed,
     prompt, gate, up, down,
     weights, wsend, pxs, pxr, xs, xr, ws, wr, hr, rr, xc, wc, acc, pt,
-    px_s, px_r, w_s, w_r, g_s, g_r, x_s, x_r, a_s, a_r, r_s, r_r, o_s, i_s, chain, normed,
+    px_s, px_r, w_s, w_r, g_s, g_r, g_f, x_s, x_r, a_s, a_r, r_s, r_r, o_s, i_s, chain, normed,
 ):
     y, x, z, c = (lax.axis_index(a) for a in ALL)
     me = 2 * z + c
@@ -133,7 +133,7 @@
     def weight_copy(t):
         return pltpu.make_async_remote_copy(
             src_ref=wsend.at[t], dst_ref=weights.at[fs, :, :, my_cols],
-            send_sem=w_s.at[t], recv_sem=w_r.at[z],
+            send_sem=w_s, recv_sem=w_r.at[z],
             device_id={"z": t}, device_id_type=MESH,
         )
 
@@ -163,17 +163,17 @@
             hear(j + 2)
             pl.when(j <= 5)(lambda: tell(j + 3))
 
-    def token_copy(tz, tc):
+    def token_copy(tz, tc, b):
         t = 2 * tz + tc
         return pltpu.make_async_remote_copy(
-            src_ref=xs.at[t], dst_ref=xr.at[me], send_sem=x_s.at[t], recv_sem=x_r.at[me],
+            src_ref=xs.at[t], dst_ref=xr.at[me], send_sem=x_s, recv_sem=x_r.at[b],
             device_id={"z": tz, "c": tc}, device_id_type=MESH,
         )
 
     def token_weight_copy(tz, tc):
         t = 2 * tz + tc
         return pltpu.make_async_remote_copy(
-            src_ref=ws.at[t], dst_ref=wr.at[me], send_sem=a_s.at[t], recv_sem=a_r.at[me],
+            src_ref=ws.at[t], dst_ref=wr.at[me], send_sem=a_s, recv_sem=a_r,
             device_id={"z": tz, "c": tc}, device_id_type=MESH,
         )
 
@@ -191,19 +191,20 @@
         col = lax.rem(z + near(k) + NZ, NZ) * 128
         return weights.at[f, :, :, pl.ds(pl.multiple_of(col, 128), 128)]
 
-    def push(k, f, ta, tb):
+    def push(k, f, ta, tb, sem):
         ax, ay = geometry(k)
         tx = lax.rem(x + ta * ax + tb * ay + NX, NX)
         ty = lax.rem(y + ta * ay + tb * ax + NY, NY)
         ref = piece(k, f)
         pltpu.make_async_remote_copy(
-            src_ref=ref, dst_ref=ref, send_sem=g_s, recv_sem=g_r.at[k, f],
+            src_ref=ref, dst_ref=ref, send_sem=g_s, recv_sem=sem,
             device_id={"y": ty, "x": tx}, device_id_type=MESH,
         ).start()
 
-    def arrived(k, f):
-        ref = piece(k, f)
-        pltpu.make_async_copy(ref, ref, g_r.at[k, f]).wait()
+    def arrived(k, stage, copies):
+        col = lax.rem(z + near(k) + NZ, NZ) * 128
+        ref = weights.at[pl.ds(0, copies), :, :, pl.ds(pl.multiple_of(col, 128), 128)]
+        pltpu.make_async_copy(ref, ref, g_r.at[k, stage]).wait()
 
     def turn(k):
         return 1 - 2 * ((k // 2) % 2)
@@ -215,14 +216,13 @@
 
     def relay(k, da):
         s = turn_of(k, da)
-        f = block(k, da, -s)
-        arrived(k, f)
-        push(k, f, 0, s)
-
-    def across(k, da):
+        push(k, block(k, da, -s), 0, s, g_f)
+
+    def across(k, da, stage):
         f = block(k, da, 0)
-        push(k, f, 0, 1)
-        push(k, f, 0, -1)
+        s = turn_of(k, da)
+        push(k, f, 0, s, g_r.at[k, stage])
+        push(k, f, 0, -s, g_f)
 
     def stage0(k):
         src = lax.rem(z + near(k) + NZ, NZ)
@@ -231,27 +231,26 @@
         def _():
             pltpu.make_async_copy(piece(k, fs), piece(k, fs), w_r.at[src]).wait()
 
-        push(k, fs, 1, 0)
-        push(k, fs, -1, 0)
-        across(k, 0)
+        push(k, fs, 1, 0, g_r.at[k, 0])
+        push(k, fs, -1, 0, g_r.at[k, 0])
+        across(k, 0, 0)
 
     def stage1(k):
         s = turn(k)
-        f = block(k, -s, 0)
-        arrived(k, f)
-        push(k, f, s, 0)
-        across(k, -s)
-        arrived(k, block(k, s, 0))
-        across(k, s)
+        arrived(k, 0, 3)
+        push(k, block(k, -s, 0), s, 0, g_r.at[k, 1])
+        across(k, -s, 1)
+        across(k, s, 1)
         relay(k, 0)
 
     def stage2(k):
-        arrived(k, block(k, 2, 0))
-        across(k, 2)
+        arrived(k, 1, 3)
+        across(k, 2, 2)
         relay(k, 1)
         relay(k, -1)
 
     def stage3(k):
+        arrived(k, 2, 1)
         relay(k, 2)
 
     def stages(step):
@@ -294,10 +293,17 @@
         tz = lax.rem(z + far(i) + NZ, NZ)
         for tc in range(2):
             token_weight_copy(tz, tc).start()
-            token_copy(tz, tc).start()
 
     token_weight_copy(z, 1 - c).start()
-    token_copy(z, 1 - c).start()
+
+    @pl.loop(0, NZ - 1)
+    def _(i):
+        tz = lax.rem(z + far(i) + NZ, NZ)
+        place = jnp.where(i > 0, i + 2 * (i % 2) - 1, 0)
+        for tc in range(2):
+            token_copy(tz, tc, place // (NZ // NB)).start()
+
+    token_copy(z, 1 - c, NB - 1).start()
     xr[me] = xs[me]
     wr[me] = ws[me]
 
@@ -312,32 +318,28 @@
     for out in outs:
         out.start()
 
-    @pl.loop(0, NZ)
-    def _(k):
-        for da in (0, 1, -1, 2):
-            s = turn_of(k, da)
-            arrived(k, block(k, da, s))
-            arrived(k, block(k, da, 2))
+    last = weights.at[pl.ds(0, 8)]
+    pltpu.make_async_copy(last, last, g_f).wait()
 
     lane = lax.broadcasted_iota(jnp.int32, (16, 128), 1)
     row = lax.broadcasted_iota(jnp.int32, (16, 128), 0)
     BZ = NZ // NB
     M = BZ * 16
 
+    def all_of(src, dst, n, sem):
+        return pltpu.make_async_copy(src.at[pl.ds(0, n)], dst.at[pl.ds(0, n)], sem)
+
+    all_of(ws, wr, NT - 1, a_r).wait()
+
     @pl.loop(0, NB)
     def _(b):
+        pl.when(b < NB - 1)(lambda: all_of(xs, xr, 2 * BZ, x_r.at[b]).wait())
+        pl.when(b == NB - 1)(lambda: all_of(xs, xr, 2 * BZ - 1, x_r.at[b]).wait())
+
         @pl.loop(0, BZ)
         def _(j):
             i = b * BZ + j
             sz = lax.rem(z + far(i) + NZ, NZ)
-            for sc in range(2):
-                t = 2 * sz + sc
-
-                @pl.when((i < NZ - 1) | (c != sc))
-                def _():
-                    pltpu.make_async_copy(xs.at[t], xr.at[t], x_r.at[t]).wait()
-                    pltpu.make_async_copy(ws.at[t], wr.at[t], a_r.at[t]).wait()
-
             at = pl.ds(pl.multiple_of(j * 16, 16), 16)
             xc[at, :] = xr[pl.ds(2 * sz, 2)].astype(F32).reshape(16, D).astype(BF)
             both = jnp.broadcast_to(wr[pl.ds(2 * sz, 2)], (2, 8, 128)).reshape(16, 128)
@@ -374,33 +376,22 @@
                 def _():
                     t = 2 * sz + sc
                     pltpu.make_async_remote_copy(
-                        src_ref=hr.at[t], dst_ref=rr.at[me], send_sem=r_s.at[t],
-                        recv_sem=r_r.at[me], device_id={"z": sz, "c": sc}, device_id_type=MESH,
+                        src_ref=hr.at[t], dst_ref=rr.at[me], send_sem=r_s,
+                        recv_sem=r_r, device_id={"z": sz, "c": sc}, device_id_type=MESH,
                     ).start()
 
     rr[me] = hr[me]
 
-    @pl.loop(1, NT)
-    def _(k):
-        t = lax.rem(me + k, NT)
-        pltpu.make_async_copy(xs.at[t], xr.at[t], x_s.at[t]).wait()
-        pltpu.make_async_copy(ws.at[t], wr.at[t], a_s.at[t]).wait()
-
-    @pl.loop(1, NZ)
-    def _(k):
-        t = lax.rem(z + k, NZ)
-        pltpu.make_async_copy(wsend.at[t], wsend.at[t], w_s.at[t]).wait()
-
+    all_of(xs, xr, NT - 1, x_s).wait()
+    all_of(ws, wr, NT - 1, a_s).wait()
+    all_of(wsend, wsend, NZ - 1, w_s).wait()
     sent = weights.at[pl.ds(0, 15)]
     pltpu.make_async_copy(sent, sent, g_s).wait()
     for out in outs:
         out.wait()
 
-    @pl.loop(1, NT)
-    def _(k):
-        t = lax.rem(me + k, NT)
-        pltpu.make_async_copy(hr.at[t], rr.at[t], r_r.at[t]).wait()
-        pltpu.make_async_copy(hr.at[t], rr.at[t], r_s.at[t]).wait()
+    all_of(hr, rr, NT - 1, r_r).wait()
+    all_of(hr, rr, NT - 1, r_s).wait()
 
     for q in range(4):
         cut = slice(512 * q, 512 * q + 512)
@@ -446,11 +437,11 @@
             pltpu.VMEM((256 // NB, D), F32),
             pltpu.VMEM((TOK, NT * CAP), BF),
             dma, dma,
-            dma((NZ,)), dma((NZ,)),
-            dma, dma((NZ, 16)),
-            dma((NT,)), dma((NT,)),
-            dma((NT,)), dma((NT,)),
-            dma((NT,)), dma((NT,)),
+            dma, dma((NZ,)),
+            dma, dma((NZ, 3)), dma,
+            dma, dma((NB,)),
+            dma, dma,
+            dma, dma,
             dma((3,)),
             dma((4,)),
             pltpu.SemaphoreType.REGULAR((2, NZ // 2 + 1)),

time: 150 us -> 146 us (0.973)
  Pallas kernels: 149 us -> 145 us
    pallas_call x1, Pallas kernels: 148 us -> 144 us  [per_device(): pl.pallas_call(body, name='relay', out_shape=(serve, serve, serve, pltpu....]
where the time goes in v4:
time: 146 us
  Pallas kernels  145 us (99%)
    pallas_call x1, Pallas kernels, per_device(): pl.pallas_call(body, name='relay', out_shape=(serve, serve, serve, pltpu....  144 us

profile of v4, /device:TPU:1, one launch (start us, length us, event | category | flops | bytes accessed | tf_op | source)
XLA Modules:
  0.0 145.9 jit_solution(6509283515777963224)
XLA Ops:
  0.6 144.1 %relay.1 = (bf16[64,2048]{1,0:T(8,128)(2,1)S(1)}, bf16[64,2048]{1,0:T(8,128)(2,1)S(1)}, bf16[64,2048]{1,0:T(8,128)(2,1)S(1)}, bf16[128,2048]{1,0:T(8,128)(2,1)S(1)}) custom-call(bf16[128,2048]{1,0:T(8,128)(2,1)} %prompt_hbm.1, s32[1,128]{1,0:T(1,128)} %bitcast.6, bf16[2,128]{1,0:T(2,128)(2,1)} %bitcast.7, f32[1,64]{1,0:T(1,128)} %bitcast.8, ...), custom_call_target="tpu_custom_call" | custom-call | tf_op jit(solution)/shard_map/relay/pallas_call | solution.py:416
  144.8 1.1 written.1

commit v5 on v4

--- a/solution.py
+++ b/solution.py
@@ -21,9 +21,9 @@
 CAP = 8
 TOK = 128
 D = 2048
-LAG1, LAG2, LAG3 = 2, 4, 6
+LAG1, LAG2, LAG3 = 3, 6, 9
 EARLY = 3
-NB = 4
+NB = 8
 
 
 def near(k):
@@ -58,7 +58,7 @@
     loads = [
         pltpu.make_async_copy(src, dst, i_s.at[n])
         for n, (src, dst) in enumerate(
-            ((prompt_hbm, prompt), (gate_hbm, gate), (up_hbm, up), (down_hbm, down))
+            ((gate_hbm, gate), (up_hbm, up), (down_hbm, down), (prompt_hbm, prompt))
         )
     ]
     for load in loads:
@@ -72,12 +72,11 @@
             value = value * gains
         return value.astype(BF)
 
-    for load in loads[1:]:
-        load.wait()
-
-    @pl.loop(0, NZ)
-    def _(t):
-        for a in range(3):
+    for a in range(3):
+        loads[a].wait()
+
+        @pl.loop(0, NZ, unroll=4)
+        def _(t):
             pxs[t, a] = rounded(a, 2 * t + 1 - c)
 
     pl.semaphore_wait(barrier, 7)
@@ -101,7 +100,7 @@
     )
     px.start()
 
-    loads[0].wait()
+    loads[3].wait()
     values = prompt[...].astype(F32)
     scale = lax.rsqrt(jnp.mean(values * values, axis=1, keepdims=True) + EPS)
     normed[...] = (values * scale).astype(BF)

time: 146 us -> 146 us (level)
  no operation moved by 1% of the time
where the time goes in v5:
time: 146 us
  Pallas kernels  145 us (99%)
    pallas_call x1, Pallas kernels, per_device(): pl.pallas_call(body, name='relay', out_shape=(serve, serve, serve, pltpu....  144 us

profile of v5, /device:TPU:1, one launch (start us, length us, event | category | flops | bytes accessed | tf_op | source)
XLA Modules:
  0.0 145.9 jit_solution(5270658816926790686)
XLA Ops:
  0.6 144.2 %relay.1 = (bf16[64,2048]{1,0:T(8,128)(2,1)S(1)}, bf16[64,2048]{1,0:T(8,128)(2,1)S(1)}, bf16[64,2048]{1,0:T(8,128)(2,1)S(1)}, bf16[128,2048]{1,0:T(8,128)(2,1)S(1)}) custom-call(bf16[128,2048]{1,0:T(8,128)(2,1)} %prompt_hbm.1, s32[1,128]{1,0:T(1,128)} %bitcast.6, bf16[2,128]{1,0:T(2,128)(2,1)} %bitcast.7, f32[1,64]{1,0:T(1,128)} %bitcast.8, ...), custom_call_target="tpu_custom_call" | custom-call | tf_op jit(solution)/shard_map/relay/pallas_call | solution.py:415
  144.8 1.1 written.1
